TPU v7x, 32 devices: a whole 2x2x4 slice. The times are simulated.
32 devices in a mesh: sp: 16 (over z, y, x), tp: 2 (over core).
Axes of the slice: x: 2, y: 2, z: 4, core: 2. Of those that a mesh axis runs over, the one named last changes fastest.
Arguments:
- out_grad: bfloat16 [3584, 2048], P('sp'), may hold values from -6 to 6
- moe_input: bfloat16 [3584, 2048], P('sp'), may hold values from -6 to 6
- routes: int32 [3584, 2], P('sp'), may hold values from 0 to 15, all different within a row; in each aligned block of 224 rows (0 to 223, 224 to 447, ...) at most 56 rows name the same one
- route_weights: float32 [3584, 2], P('sp'), may hold values from 0.2 to 1
- conv_result: bfloat16 [3584, 1024], P('sp', 'tp'), may hold values from -60 to 60
- glu_value: bfloat16 [3584, 1024], P('sp', 'tp'), may hold values from -6 to 6
- glu_gate: bfloat16 [3584, 1024], P('sp', 'tp'), may hold values from -6 to 6
- conv_taps: bfloat16 [31, 1024], P(None, 'tp'), may hold values from -1 to 1
- norm_gain: float32 [1024], P('tp'), may hold values from 0.1 to 1.9
- proj_weight: bfloat16 [2048, 1024], P(None, 'tp'), may hold values from -0.1875 to 0.1875
- expert_gate: bfloat16 [16, 2048, 1024], P('sp', None, 'tp'), may hold values from -0.125 to 0.125
- expert_up: bfloat16 [16, 2048, 1024], P('sp', None, 'tp'), may hold values from -0.125 to 0.125
- expert_down: bfloat16 [16, 1024, 2048], P('sp', 'tp'), may hold values from -0.1875 to 0.1875
Outputs:
- input_grad: bfloat16 [3584, 2048], P('sp')
- proj_grad: float32 [2048, 1024], P('sp', 'tp')
- gate_grad: float32 [16, 2048, 1024], P('sp', None, 'tp')
- up_grad: float32 [16, 2048, 1024], P('sp', None, 'tp')
- down_grad: float32 [16, 1024, 2048], P('sp', 'tp')
- value_grad: bfloat16 [3584, 1024], P('sp', 'tp')
- gate_side_grad: bfloat16 [3584, 1024], P('sp', 'tp')
Inputs may be any that keep to these rules, and one draw needn't show every extreme that they name: `routes`: in each aligned block of 224 tokens no expert is named more than 56 times, a bound that some block reaches; a token's experts differ.
All inputs are finite; a program needn't handle non-finite values.
Results may differ from a plain program's by a relative error of at most 0.0061.
Values may be sent and summed in bfloat16 or wider, within the bound.
A program may use at most 128 MiB of HBM per device.

v0:
```python
import jax
import jax.numpy as jnp
from jax import lax
from jax.sharding import PartitionSpec as P

norm_eps = 1e-05


def from_behind(shard, axis, by):
    count = lax.axis_size(axis)
    pairs = [(i, i + by) for i in range(count) if 0 <= i + by < count]
    return lax.ppermute(shard, axis, pairs)


def contract_rows(left, right):
    return lax.dot_general(
        left, right, (((0,), (0,)), ((), ())), preferred_element_type=jnp.float32
    )


def contract_cols(left, right):
    return lax.dot_general(
        left, right, (((1,), (1,)), ((), ())), preferred_element_type=jnp.float32
    )


def per_device(
    out_grad,
    moe_input,
    routes,
    route_weights,
    conv_result,
    glu_value,
    glu_gate,
    conv_taps,
    norm_gain,
    proj_weight,
    expert_gate,
    expert_up,
    expert_down,
):
    n_sp = lax.axis_size("sp")
    n_tp = lax.axis_size("tp")
    tok_rows, width = out_grad.shape
    top_count = routes.shape[1]
    capacity = 2 * top_count * tok_rows // n_sp
    slots = n_sp * capacity
    assigned = tok_rows * top_count
    values = conv_result.astype(jnp.float32)
    channels = conv_result.shape[1] * n_tp
    sums, squares = lax.psum((jnp.sum(values, axis=1), jnp.sum(values * values, axis=1)), "tp")
    center = sums / channels
    spread = squares / channels - center * center
    inv_std = lax.rsqrt(spread + norm_eps)[:, None]
    normed = (values - center[:, None]) * inv_std
    scaled = normed * norm_gain[None, :]
    sig_norm = jax.nn.sigmoid(scaled)
    activ = (scaled * sig_norm).astype(jnp.bfloat16)
    expert_flat = routes.reshape(assigned)
    onehot = (expert_flat[:, None] == jnp.arange(n_sp, dtype=jnp.int32)[None, :]).astype(jnp.int32)
    earlier = jnp.cumsum(onehot, axis=0) - onehot
    slot_index = jnp.sum(earlier * onehot, axis=1)
    target = expert_flat * capacity + slot_index
    source = (
        jnp.full((slots,), assigned, jnp.int32)
        .at[target]
        .set(jnp.arange(assigned, dtype=jnp.int32))
    )
    token = jnp.where(source < assigned, source // top_count, tok_rows)
    grad_padded = jnp.concatenate([out_grad, jnp.zeros((1, width), jnp.bfloat16)], axis=0)
    input_padded = jnp.concatenate([moe_input, jnp.zeros((1, width), jnp.bfloat16)], axis=0)
    weight_padded = jnp.concatenate([route_weights.reshape(assigned), jnp.zeros((1,), jnp.float32)])
    send_input = input_padded[token]
    send_grad = (grad_padded[token].astype(jnp.float32) * weight_padded[source][:, None]).astype(
        jnp.bfloat16
    )
    row_scale = float(slots) ** (-0.5)
    share = width // n_tp
    offset = lax.axis_index("tp") * share
    input_share = lax.dynamic_slice_in_dim(send_input, offset, share, 1)
    grad_share = lax.dynamic_slice_in_dim(send_grad, offset, share, 1)
    input_part, grad_part = (
        lax.all_to_all(input_share, "sp", split_axis=0, concat_axis=0, tiled=True),
        lax.all_to_all(grad_share, "sp", split_axis=0, concat_axis=0, tiled=True),
    )
    inputs, grads = (
        lax.all_gather(input_part, "tp", axis=1, tiled=True),
        lax.all_gather(grad_part, "tp", axis=1, tiled=True),
    )
    gate_pre = jnp.dot(inputs, expert_gate[0], preferred_element_type=jnp.float32)
    up_pre = jnp.dot(inputs, expert_up[0], preferred_element_type=jnp.float32)
    sigma = jax.nn.sigmoid(gate_pre)
    silu_gate = gate_pre * sigma
    hidden = (silu_gate * up_pre).astype(jnp.bfloat16)
    down_g = contract_rows(hidden, grads) * row_scale
    hidden_grad = contract_cols(grads, expert_down[0])
    gate_back = (hidden_grad * up_pre * sigma * (1.0 + gate_pre * (1.0 - sigma))).astype(
        jnp.bfloat16
    )
    up_back = (hidden_grad * silu_gate).astype(jnp.bfloat16)
    gate_g = contract_rows(inputs, gate_back) * row_scale
    up_g = contract_rows(inputs, up_back) * row_scale
    partial_value = contract_cols(gate_back, expert_gate[0]) + contract_cols(up_back, expert_up[0])
    gate_g, up_g, down_g, partial_value = (gate_g, up_g, down_g, partial_value)
    summed = lax.psum_scatter(
        partial_value.astype(jnp.bfloat16), "tp", scatter_dimension=1, tiled=True
    )
    returned_part = lax.all_to_all(summed, "sp", split_axis=0, concat_axis=0, tiled=True)
    returned = lax.all_gather(returned_part, "tp", axis=1, tiled=True)
    contrib = returned[target].reshape(tok_rows, top_count, width).astype(jnp.float32)
    input_grad = (out_grad.astype(jnp.float32) + jnp.sum(contrib, axis=1)).astype(jnp.bfloat16)
    token_scale = float(tok_rows * n_sp) ** (-0.5)
    proj_grad = lax.psum_scatter(
        contract_rows(input_grad, activ) * token_scale, "sp", scatter_dimension=0, tiled=True
    )
    act_grad = jnp.dot(input_grad, proj_weight, preferred_element_type=jnp.float32)
    norm_grad = act_grad * sig_norm * (1.0 + scaled * (1.0 - sig_norm)) * norm_gain[None, :]
    first, second = lax.psum(
        (jnp.sum(norm_grad, axis=1), jnp.sum(norm_grad * normed, axis=1)), "tp"
    )
    conv_grad = inv_std * (
        norm_grad - first[:, None] / channels - normed * (second[:, None] / channels)
    )
    reach = conv_taps.shape[0]
    rim = from_behind(conv_grad[: reach - 1].astype(jnp.bfloat16), "sp", -1).astype(jnp.float32)
    extended = jnp.concatenate([conv_grad, rim], axis=0)
    taps_float = conv_taps.astype(jnp.float32)
    mixed_grad = jnp.zeros_like(conv_grad)
    for lag in range(reach):
        mixed_grad = (
            mixed_grad + taps_float[reach - 1 - lag][None, :] * extended[lag : lag + tok_rows]
        )
    sig_gate = jax.nn.sigmoid(glu_gate.astype(jnp.float32))
    value_grad = (mixed_grad * sig_gate).astype(jnp.bfloat16)
    gate_side_grad = (
        mixed_grad * glu_value.astype(jnp.float32) * sig_gate * (1.0 - sig_gate)
    ).astype(jnp.bfloat16)
    return (
        input_grad,
        proj_grad,
        gate_g[None],
        up_g[None],
        down_g[None],
        value_grad,
        gate_side_grad,
    )


def solution(mesh):
    in_specs = (
        P("sp", None),
        P("sp", None),
        P("sp", None),
        P("sp", None),
        P("sp", "tp"),
        P("sp", "tp"),
        P("sp", "tp"),
        P(None, "tp"),
        P("tp"),
        P(None, "tp"),
        P("sp", None, "tp"),
        P("sp", None, "tp"),
        P("sp", "tp", None),
    )
    out_specs = (
        P("sp", None),
        P("sp", "tp"),
        P("sp", None, "tp"),
        P("sp", None, "tp"),
        P("sp", "tp", None),
        P("sp", "tp"),
        P("sp", "tp"),
    )
    return jax.shard_map(
        per_device, mesh=mesh, in_specs=in_specs, out_specs=out_specs, check_vma=False
    )
```

profile of v0, /device:TPU:0, one launch (start us, length us, event | category | flops | bytes accessed | tf_op | source)
XLA Modules:
  0.0 347.4 jit_solution(11631371816840347325)
XLA Ops:
  7.2 0.9 copy.21
  8.1 0.7 broadcast_multiply_fusion
  8.8 0.1 eq.22
  9.0 1.2 reduce-window.6
  10.2 0.2 slice_reduce_fusion
  10.5 0.1 copy.20
  10.7 0.1 mul.450
  10.8 2.9 scatter_custom_fusion
  13.8 1.2 concatenate.14
  15.0 5.0 %gather_fusion.2 = bf16[896,2048]{1,0:T(8,128)(2,1)} fusion(bf16[225,2048]{1,0:T(8,128)(2,1)S(1)} %concatenate.14, s32[1024]{0:T(1024)S(1)} %get-tuple-element.56), kind=kCustom, calls=%fused_computation.2 | custom fusion | bytes 7343616 | tf_op jit(solution)/shard_map/gather | solution.py:73
  20.0 2.9 constant_dynamic-slice_fusion
  22.9 8.4 %all-to-all-start.1 = ((bf16[16,56,1024]{2,1,0:T(8,128)(2,1)}), bf16[16,56,1024]{2,1,0:T(8,128)(2,1)}, u32[]{:S(2)}, u32[]{:S(2)}) async-start(bf16[16,56,1024]{2,1,0:T(8,128)(2,1)} %bitcast.88), calls=%async_computation.1 | async-start | bytes 3670016 | tf_op jit(solution)/shard_map/all_to_all | solution.py:83
  31.3 1.2 concatenate.12
  32.6 5.0 %gather_fusion = bf16[896,2048]{1,0:T(8,128)(2,1)} fusion(bf16[225,2048]{1,0:T(8,128)(2,1)S(1)} %concatenate.12, s32[1024]{0:T(1024)S(1)} %get-tuple-element.56), kind=kCustom, calls=%fused_computation | custom fusion | bytes 7343616 | tf_op jit(solution)/shard_map/gather | solution.py:74
  37.7 0.1 reshape.77
  37.9 5.8 %gather_fusion.1 = f32[896]{0:T(1024)S(1)} fusion(f32[449]{0:T(512)S(1)} %pad_maximum_fusion.1, s32[1024]{0:T(1024)S(1)} %get-tuple-element.55), kind=kCustom, calls=%fused_computation.1 | custom fusion | bytes 10752 | tf_op jit(solution)/shard_map/gather | solution.py:74
  43.7 26.2 %all-to-all-done.1 = bf16[16,56,1024]{2,1,0:T(8,128)(2,1)} async-done(((bf16[16,56,1024]{2,1,0:T(8,128)(2,1)}), bf16[16,56,1024]{2,1,0:T(8,128)(2,1)}, u32[]{:S(2)}, u32[]{:S(2)}) %all-to-all-start.1) | async-done | bytes 1835040 | tf_op jit(solution)/shard_map/all_to_all | solution.py:83
  69.9 1.9 multiply_convert_fusion
  71.8 51.9 %all_to_all.36 = bf16[16,56,1024]{2,1,0:T(8,128)(2,1)} all-to-all(bf16[16,56,1024]{2,1,0:T(8,128)(2,1)S(1)} %bitcast.87), channel_id=1, replica_groups=mesh['sp'=16,'tp'=2] {'sp'}, dimensions={0} | all-to-all | bytes 3670016 | tf_op jit(solution)/shard_map/all_to_all | solution.py:84
  123.7 0.2 reduce-scatter.3.cloned.1.call-start
  124.0 5.5 %fusion.2 = f32[896,512]{1,0:T(8,128)} fusion(bf16[896,2048]{1,0:T(8,128)(2,1)} %all-gather.6.cloned.1.call-done, bf16[1,2048,512]{2,1,0:T(8,128)(2,1)S(1)} %copy-done), kind=kOutput, calls=%fused_computation.42 | convolution fusion | flops 1879048192 | bytes 7602176 | tf_op jit(solution)/shard_map/dot_general | solution.py:90
  129.5 3.4 fusion.5
  132.9 1.7 all-gather.4.cloned.1.call-done
  134.6 6.4 %multiply_convert_fusion.2 = (bf16[896,512]{1,0:T(8,128)(2,1)S(1)}, bf16[896,512]{1,0:T(8,128)(2,1)S(1)}) fusion(f32[896,512]{1,0:T(8,128)} %fusion.2, f32[896,512]{1,0:T(8,128)} %fusion.5, bf16[896,2048]{1,0:T(8,128)(2,1)} %all-gather.4.cloned.1.call-done, bf16[1,512,2048]{2,1,0:T(8,128)(2,1)} %param.25), kind=kOutput, calls=%fused_computation.51 | convolution fusion | flops 1885011968 | bytes 11272192 | tf_op jit(solution)/shard_map/dot_general | solution.py:22
  141.0 2.1 fusion
  143.2 3.9 %add_convert_fusion = bf16[896,2048]{1,0:T(8,128)(2,1)} fusion(f32[896,2048]{1,0:T(8,128)S(1)} %fusion, bf16[896,512]{1,0:T(8,128)(2,1)S(1)} %get-tuple-element.17, bf16[1,2048,512]{2,1,0:T(8,128)(2,1)S(1)} %copy-done.4), kind=kOutput, calls=%fused_computation.5 | convolution fusion | flops 1882718208 | bytes 14024704 | tf_op jit(solution)/shard_map/dot_general | solution.py:22
  147.2 12.9 %reduce-scatter.3.cloned.1.call-done = bf16[896,1024]{1,0:T(8,128)(2,1)} async-done(((bf16[896,2048]{1,0:T(8,128)(2,1)}), bf16[896,1024]{1,0:T(8,128)(2,1)}) %reduce-scatter.3.cloned.1.call-update) | async-done | bytes 1835024 | tf_op jit(solution)/shard_map/reduce_scatter | solution.py:105
  160.1 51.2 %all_to_all.37 = bf16[16,56,1024]{2,1,0:T(8,128)(2,1)} all-to-all(bf16[16,56,1024]{2,1,0:T(8,128)(2,1)} %bitcast.89), channel_id=1, replica_groups=mesh['sp'=16,'tp'=2] {'sp'}, dimensions={0} | all-to-all | bytes 3670016 | tf_op jit(solution)/shard_map/all_to_all | solution.py:108
  211.4 0.2 convert_reduce_fusion
  211.6 2.5 all-reduce.4
  214.1 8.1 %all-gather.8.cloned.1.call-done = bf16[896,2048]{1,0:T(8,128)(2,1)} async-done(((bf16[896,1024]{1,0:T(8,128)(2,1)}), bf16[896,2048]{1,0:T(8,128)(2,1)}) %all-gather.8.cloned.1.call-update) | async-done | bytes 3670032 | tf_op jit(solution)/shard_map/all_gather | solution.py:109
  222.2 6.9 %gather_fusion.3 = bf16[448,2048]{1,0:T(8,128)(2,1)S(1)} fusion(bf16[896,2048]{1,0:T(8,128)(2,1)} %all-gather.8.cloned.1.call-done, s32[1024]{0:T(1024)S(1)} %pad_clamp_fusion), kind=kCustom, calls=%fused_computation.3 | custom fusion | bytes 3671808 | tf_op jit(solution)/shard_map/gather | solution.py:110
  229.1 3.5 %reshape.79 = f32[224,2,2048]{2,1,0:T(2,128)} reshape(bf16[448,2048]{1,0:T(8,128)(2,1)S(1)} %gather_fusion.3) | data formatting | bytes 5505024 | tf_op jit(solution)/shard_map/convert_element_type | solution.py:110
  232.6 6.5 %reduce_sum.58 = f32[224,2048]{1,0:T(8,128)S(1)} reduce(f32[224,2,2048]{2,1,0:T(2,128)} %reshape.79, f32[]{:T(128)} %constant.61.clone.1), dimensions={1}, to_apply=%region_5.6 | reduce | flops 458752 | bytes 5505028 | tf_op jit(solution)/shard_map/reduce_sum | solution.py:111
  239.1 1.4 add_convert_fusion.1
  240.5 3.0 convolution_multiply_fusion
  243.6 0.7 copy-done.10
  244.4 0.4 copy-done.8
  244.7 6.6 %multiply_bitcast_fusion.1 = f32[1,2048,512]{2,1,0:T(8,128)} fusion(bf16[896,2048]{1,0:T(8,128)(2,1)} %all-gather.6.cloned.1.call-done, bf16[896,512]{1,0:T(8,128)(2,1)S(1)} %copy-done.8), kind=kOutput, calls=%fused_computation.36 | convolution fusion | flops 1880096768 | bytes 8781824 | tf_op jit(solution)/shard_map/dot_general | solution.py:16
  251.4 4.6 %multiply_bitcast_fusion = f32[1,512,2048]{2,1,0:T(8,128)} fusion(bf16[896,2048]{1,0:T(8,128)(2,1)S(1)} %copy-done.14, f32[896,512]{1,0:T(8,128)S(1)} %copy-done.18, f32[896,512]{1,0:T(8,128)S(1)} %copy-done.17), kind=kOutput, calls=%fused_computation.35 | convolution fusion | flops 1882849280 | bytes 11534336 | tf_op jit(solution)/shard_map/dot_general | solution.py:16
  255.9 0.9 fusion.132
  256.8 2.5 all-reduce.3
  259.3 0.2 fusion.114
  259.5 1.7 collective-permute-start
  261.2 6.8 %multiply_bitcast_fusion.2 = f32[1,2048,512]{2,1,0:T(8,128)} fusion(bf16[896,2048]{1,0:T(8,128)(2,1)} %all-gather.6.cloned.1.call-done, bf16[896,512]{1,0:T(8,128)(2,1)} %copy-done.16), kind=kOutput, calls=%fused_computation.37 | convolution fusion | flops 1880096768 | bytes 8781824 | tf_op jit(solution)/shard_map/dot_general | solution.py:16
  268.1 3.1 multiply_convert_fusion.5
  271.1 0.8 multiply_convert_fusion.6
  272.0 68.9 %reduce-scatter.5.cloned.1.call-done = f32[128,512]{1,0:T(8,128)} async-done(((f32[2048,512]{1,0:T(8,128)}), f32[128,512]{1,0:T(8,128)}) %reduce-scatter.5.cloned.1.call-update) | async-done | bytes 262160 | tf_op jit(solution)/shard_map/reduce_scatter | solution.py:113
  (67 shorter events, 1.0 us)
Async XLA Ops:
  7.2 116.8 %copy-start = (bf16[1,2048,512]{2,1,0:T(8,128)(2,1)S(1)}, bf16[1,2048,512]{2,1,0:T(8,128)(2,1)}, u32[]{:S(2)}) copy-start(bf16[1,2048,512]{2,1,0:T(8,128)(2,1)} %param.23) | copy-start | bytes 6291460
  22.9 47.0 %all-to-all-start.1 = ((bf16[16,56,1024]{2,1,0:T(8,128)(2,1)}), bf16[16,56,1024]{2,1,0:T(8,128)(2,1)}, u32[]{:S(2)}, u32[]{:S(2)}) async-start(bf16[16,56,1024]{2,1,0:T(8,128)(2,1)} %bitcast.88), calls=%async_computation.1 | async-start | bytes 3670016 | tf_op jit(solution)/shard_map/all_to_all | solution.py:83
  31.3 92.7 %all-gather.6.cloned.1.call-start = ((), (), s32[]{:S(2)}) async-start(), calls=%async_computation.6 | async-start | bytes 5505024 | tf_op jit(solution)/shard_map/all_gather | solution.py:87
  32.6 5.0 %copy-start.11 = (f32[224,2]{0,1:T(2,128)S(1)}, f32[224,2]{0,1:T(2,128)}, u32[]{:S(2)}) copy-start(f32[224,2]{0,1:T(2,128)} %param.16) | copy-start | bytes 5380
  69.9 64.7 %all-gather.4.cloned.1.call-start = ((), (), s32[]{:S(2)}) async-start(), calls=%async_computation.5 | async-start | bytes 5505024 | tf_op jit(solution)/shard_map/all_gather | solution.py:88
  123.7 36.4 %reduce-scatter.3.cloned.1.call-start = ((), (), s32[]{:S(2)}) async-start(), calls=%async_computation.7 | async-start | bytes 5505024 | tf_op jit(solution)/shard_map/reduce_scatter | solution.py:105
  124.0 5.5 %copy-start.3 = (bf16[1,2048,512]{2,1,0:T(8,128)(2,1)S(1)}, bf16[1,2048,512]{2,1,0:T(8,128)(2,1)}, u32[]{:S(2)}) copy-start(bf16[1,2048,512]{2,1,0:T(8,128)(2,1)} %param.24) | copy-start | bytes 6291460
  124.0 5.5 %copy-start.13 = (bf16[896,2048]{1,0:T(8,128)(2,1)S(1)}, bf16[896,2048]{1,0:T(8,128)(2,1)}, u32[]{:S(2)}) copy-start(bf16[896,2048]{1,0:T(8,128)(2,1)} %all-gather.6.cloned.1.call-done) | copy-start | bytes 11010052
  141.0 2.1 copy-start.16
  141.0 2.1 copy-start.7
  141.0 2.3 copy-start.4
  147.2 75.0 %all-gather.8.cloned.1.call-start = ((), (), s32[]{:S(2)}) async-start(), calls=%async_computation.8 | async-start | bytes 5505024 | tf_op jit(solution)/shard_map/all_gather | solution.py:109
  160.1 51.3 %copy-start.5 = (bf16[224,512]{1,0:T(8,128)(2,1)S(1)}, bf16[224,512]{1,0:T(8,128)(2,1)}, u32[]{:S(2)}) copy-start(bf16[224,512]{1,0:T(8,128)(2,1)} %param.17) | copy-start | bytes 688132
  211.4 129.5 %reduce-scatter.5.cloned.1.call-start = ((), (), s32[]{:S(2)}) async-start(), calls=%async_computation.9 | async-start | bytes 4456448 | tf_op jit(solution)/shard_map/reduce_scatter | solution.py:113
  239.1 1.4 copy-start.12
  240.5 15.4 %copy-start.2 = (bf16[224,2048]{1,0:T(8,128)(2,1)}, bf16[224,2048]{1,0:T(8,128)(2,1)S(1)}, u32[]{:S(2)}) copy-start(bf16[224,2048]{1,0:T(8,128)(2,1)S(1)} %add_convert_fusion.1) | copy-start | bytes 2752516
  243.5 0.8 copy-start.10
  243.5 1.2 copy-start.8
  244.7 6.6 %copy-start.14 = (bf16[896,2048]{1,0:T(8,128)(2,1)S(1)}, bf16[896,2048]{1,0:T(8,128)(2,1)}, u32[]{:S(2)}) copy-start(bf16[896,2048]{1,0:T(8,128)(2,1)} %all-gather.4.cloned.1.call-done) | copy-start | bytes 11010052
  244.7 6.6 %copy-start.17 = (f32[896,512]{1,0:T(8,128)S(1)}, f32[896,512]{1,0:T(8,128)}, u32[]{:S(2)}) copy-start(f32[896,512]{1,0:T(8,128)} %fusion.2) | copy-start | bytes 5505028
  244.7 6.6 %copy-start.18 = (f32[896,512]{1,0:T(8,128)S(1)}, f32[896,512]{1,0:T(8,128)}, u32[]{:S(2)}) copy-start(f32[896,512]{1,0:T(8,128)} %fusion.5) | copy-start | bytes 5505028
  251.3 4.6 %copy-start.15 = (bf16[2048,512]{1,0:T(8,128)(2,1)S(1)}, bf16[2048,512]{1,0:T(8,128)(2,1)}, u32[]{:S(2)}) copy-start(bf16[2048,512]{1,0:T(8,128)(2,1)} %param.22) | copy-start | bytes 6291460
  259.5 8.6 %copy-start.6 = (bf16[224,512]{1,0:T(8,128)(2,1)S(1)}, bf16[224,512]{1,0:T(8,128)(2,1)}, u32[]{:S(2)}) copy-start(bf16[224,512]{1,0:T(8,128)(2,1)} %param.19) | copy-start | bytes 688132
  259.5 8.6 %copy-start.9 = (bf16[224,512]{1,0:T(8,128)(2,1)S(1)}, bf16[224,512]{1,0:T(8,128)(2,1)}, u32[]{:S(2)}) copy-start(bf16[224,512]{1,0:T(8,128)(2,1)} %param.18) | copy-start | bytes 688132
  259.5 8.6 %collective-permute-start = (bf16[30,512]{1,0:T(8,128)(2,1)S(1)}, bf16[30,512]{1,0:T(8,128)(2,1)S(1)}, u32[]{:S(2)}, u32[]{:S(2)}) collective-permute-start(bf16[30,512]{1,0:T(8,128)(2,1)S(1)} %slice.760), channel_id=1, source_target_pairs={{2,0},{4,2},{6,4},{8,6},{10,8},{12,10},{14,12},{16,14},{18,16},{20... | collective-permute-start | bytes 92168 | tf_op jit(solution)/shard_map/ppermute | solution.py:12
  261.2 79.7 %copy-start.1 = (bf16[1,2048,512]{2,1,0:T(8,128)(2,1)S(1)}, bf16[1,2048,512]{2,1,0:T(8,128)(2,1)}, u32[]{:S(2)}) copy-start(bf16[1,2048,512]{2,1,0:T(8,128)(2,1)} %param.23) | copy-start | bytes 6291460
Sparse Core Ops, SparseCore 0:
  70.0 16.1 all-gather.5
  123.9 10.6 all-gather.3
  147.3 12.7 reduce-scatter.2
  211.5 10.6 all-gather.7
  243.7 97.1 reduce-scatter.4
where the time goes:
time: 348 us; the launch traced here: 347 us
  waiting for transfers between devices  118 us (34%)
  blocking collectives  108 us (31%)
  matrix products  43.1 us (12%)
  local copies, waits for them, and re-layouts  37.6 us (11%)
  other arithmetic  16.1 us (5%)
  between operations  14.2 us (4%)
  starting transfers between devices  10.5 us (3%)
    reduce_scatter x1, waiting for transfers between devices, per_device(): lax.psum_scatter(contract_rows(input_grad, activ) * token_scale, 'sp', sc...  68.9 us
    all_to_all x1, blocking collectives, per_device(): lax.all_to_all(grad_share, 'sp', split_axis=0, concat_axis=0, tiled=True)  51.9 us
    all_to_all x1, blocking collectives, per_device(): lax.all_to_all(summed, 'sp', split_axis=0, concat_axis=0, tiled=True)  51.2 us
    all_to_all x1, waiting for transfers between devices, per_device(): lax.all_to_all(input_share, 'sp', split_axis=0, concat_axis=0, tiled=True)  26.2 us
    dot_general x4, matrix products, contract_rows(): lax.dot_general(left, right, (((0,), (0,)), ((), ())), preferred_element_...  21 us
    reduce_scatter x1, waiting for transfers between devices, per_device(): lax.psum_scatter(partial_value.astype(jnp.bfloat16), 'tp', scatter_dimens...  12.9 us
    dot_general x3, matrix products, contract_cols(): lax.dot_general(left, right, (((1,), (1,)), ((), ())), preferred_element_...  12.4 us
    all_to_all x1, starting transfers between devices, per_device(): lax.all_to_all(input_share, 'sp', split_axis=0, concat_axis=0, tiled=True)  8.39 us
  transfers between devices with their start and end apart: 7, of which 5 were waited for; matrix products, arithmetic and copies ran while one was open for 13% of the time, Pallas kernels for 0%

commit v1 on v0

v1 whole, which is shorter than its diff:
```python
import functools

import jax
import jax.numpy as jnp
from jax import lax
from jax.experimental import pallas as pl
from jax.experimental.pallas import tpu as pltpu
from jax.sharding import PartitionSpec as P

norm_eps = 1e-05
MESH = pl.DeviceIdType.MESH


def from_behind(shard, axis, by):
    count = lax.axis_size(axis)
    pairs = [(i, i + by) for i in range(count) if 0 <= i + by < count]
    return lax.ppermute(shard, axis, pairs)


def contract_rows(left, right):
    return lax.dot_general(
        left, right, (((0,), (0,)), ((), ())), preferred_element_type=jnp.float32
    )


def contract_cols(left, right):
    return lax.dot_general(
        left, right, (((1,), (1,)), ((), ())), preferred_element_type=jnp.float32
    )


def exchange_body(n, number, relay, lanes, *refs):
    xs, outs = refs[:number], refs[number : 2 * number]
    own_sem, send_sem, recv_sem = refs[2 * number : 2 * number + 3]
    fwd_send, fwd_recv = refs[2 * number + 3 :] if relay else (None, None)
    me = lax.axis_index("sp")
    half = lax.axis_index("tp")
    other = 1 - half

    def place(a, source, side):
        if not relay:
            return outs[a].at[source]
        if lanes:
            cols = xs[a].shape[2]
            return outs[a].at[source, :, pl.ds(pl.multiple_of(side * cols, cols), cols)]
        return outs[a].at[side, source]

    def outgoing(a, step):
        peer = lax.rem(me + step, n)
        return pltpu.make_async_remote_copy(
            src_ref=xs[a].at[peer],
            dst_ref=place(a, me, half),
            send_sem=send_sem.at[a, step],
            recv_sem=recv_sem.at[a, step],
            device_id=(peer, half),
            device_id_type=MESH,
        )

    def incoming(a, step):
        peer = lax.rem(me + step, n)
        source = lax.rem(me + n - step, n)
        return pltpu.make_async_remote_copy(
            src_ref=xs[a].at[peer],
            dst_ref=place(a, source, half),
            send_sem=send_sem.at[a, step],
            recv_sem=recv_sem.at[a, step],
            device_id=(peer, half),
            device_id_type=MESH,
        )

    def relayed(a, step, first=False):
        source = lax.rem(me + n - step, n)
        return pltpu.make_async_remote_copy(
            src_ref=xs[a].at[me] if first else place(a, source, half),
            dst_ref=place(a, source, half),
            send_sem=fwd_send.at[a, step],
            recv_sem=fwd_recv.at[a, step],
            device_id=(me, other),
            device_id_type=MESH,
        )

    def from_other(a, step):
        source = lax.rem(me + n - step, n)
        return pltpu.make_async_remote_copy(
            src_ref=xs[a].at[me],
            dst_ref=place(a, source, other),
            send_sem=fwd_send.at[a, step],
            recv_sem=fwd_recv.at[a, step],
            device_id=(me, other),
            device_id_type=MESH,
        )

    barrier = pltpu.get_barrier_semaphore()

    def greet(step, carry):
        pl.semaphore_signal(
            barrier, inc=1, device_id=(lax.rem(me + step, n), half), device_id_type=MESH
        )
        return carry

    lax.fori_loop(1, n, greet, 0)
    if relay:
        pl.semaphore_signal(barrier, inc=1, device_id=(me, other), device_id_type=MESH)
    pl.semaphore_wait(barrier, n - 1 + (1 if relay else 0))

    for a in range(number):

        def send(step, carry, a=a):
            outgoing(a, step).start()
            return carry

        lax.fori_loop(1, n, send, 0)
    own = []
    for a in range(number):
        own.append(pltpu.make_async_copy(xs[a].at[me], place(a, me, half), own_sem.at[a]))
        own[-1].start()
        if relay:
            relayed(a, 0, first=True).start()
    for a in range(number):

        def arrive(step, carry, a=a):
            incoming(a, step).wait_recv()
            if relay:
                relayed(a, step).start()
            return carry

        lax.fori_loop(1, n, arrive, 0)
    for a in range(number):

        def finish(step, carry, a=a):
            outgoing(a, step).wait_send()
            if relay:
                relayed(a, step).wait_send()
                from_other(a, step).wait_recv()
            return carry

        lax.fori_loop(1, n, finish, 0)
        own[a].wait()
        if relay:
            relayed(a, 0, first=True).wait_send()
            from_other(a, 0).wait_recv()


def exchange(arrays, collective_id, relay=True, lanes=True):
    n = lax.axis_size("sp")
    number = len(arrays)
    outs = []
    for x in arrays:
        shape = x.shape
        if relay:
            shape = (shape[0], shape[1], 2 * shape[2]) if lanes else (2,) + shape
        outs.append(jax.ShapeDtypeStruct(shape, x.dtype))
    sems = [pltpu.SemaphoreType.DMA((number,))] + [pltpu.SemaphoreType.DMA((number, n))] * (
        4 if relay else 2
    )
    return pl.pallas_call(
        functools.partial(exchange_body, n, number, relay, lanes),
        out_shape=tuple(outs),
        in_specs=[pl.BlockSpec(memory_space=pltpu.VMEM)] * number,
        out_specs=tuple([pl.BlockSpec(memory_space=pl.ANY)] * number),
        scratch_shapes=sems,
        compiler_params=pltpu.CompilerParams(collective_id=collective_id, has_side_effects=True),
    )(*arrays)


def per_device(
    out_grad,
    moe_input,
    routes,
    route_weights,
    conv_result,
    glu_value,
    glu_gate,
    conv_taps,
    norm_gain,
    proj_weight,
    expert_gate,
    expert_up,
    expert_down,
):
    n_sp = lax.axis_size("sp")
    n_tp = lax.axis_size("tp")
    half = lax.axis_index("tp")
    tok_rows, width = out_grad.shape
    top_count = routes.shape[1]
    capacity = 2 * top_count * tok_rows // n_sp
    slots = n_sp * capacity
    share = width // n_tp
    experts = jnp.arange(n_sp, dtype=jnp.int32)[None, :]
    named = [(routes[:, k : k + 1] == experts) for k in range(top_count)]
    per_token = sum(hit.astype(jnp.bfloat16) for hit in named)
    order = jnp.arange(tok_rows, dtype=jnp.int32)
    before = (order[None, :] < order[:, None]).astype(jnp.bfloat16)
    earlier = jnp.dot(before, per_token, preferred_element_type=jnp.float32).astype(jnp.int32)
    rows = jnp.arange(slots, dtype=jnp.int32)
    chosen = []
    for k in range(top_count):
        slot = jnp.sum(jnp.where(named[k], earlier, 0), axis=1)
        target = routes[:, k] * capacity + slot
        chosen.append(rows[:, None] == target[None, :])
    pick = functools.reduce(jnp.logical_or, chosen).astype(jnp.bfloat16)
    row_weight = sum(
        jnp.sum(jnp.where(chosen[k], route_weights[:, k][None, :], 0.0), axis=1)
        for k in range(top_count)
    )
    input_half = lax.dynamic_slice_in_dim(moe_input, half * share, share, 1)
    grad_half = lax.dynamic_slice_in_dim(out_grad, half * share, share, 1)
    send_input = jnp.dot(pick, input_half, preferred_element_type=jnp.float32).astype(jnp.bfloat16)
    send_grad = (
        jnp.dot(pick, grad_half, preferred_element_type=jnp.float32) * row_weight[:, None]
    ).astype(jnp.bfloat16)
    row_scale = float(slots) ** (-0.5)
    blocks = (n_sp, capacity, share)
    inputs, grads = exchange([send_input.reshape(blocks), send_grad.reshape(blocks)], 1)
    inputs, grads = inputs.reshape(slots, width), grads.reshape(slots, width)

    values = conv_result.astype(jnp.float32)
    channels = conv_result.shape[1] * n_tp
    sums, squares = lax.psum((jnp.sum(values, axis=1), jnp.sum(values * values, axis=1)), "tp")
    center = sums / channels
    spread = squares / channels - center * center
    inv_std = lax.rsqrt(spread + norm_eps)[:, None]
    normed = (values - center[:, None]) * inv_std
    scaled = normed * norm_gain[None, :]
    sig_norm = jax.nn.sigmoid(scaled)
    activ = (scaled * sig_norm).astype(jnp.bfloat16)
    all_activ = lax.all_gather(activ, "sp", axis=0, tiled=True)

    gate_pre = jnp.dot(inputs, expert_gate[0], preferred_element_type=jnp.float32)
    up_pre = jnp.dot(inputs, expert_up[0], preferred_element_type=jnp.float32)
    sigma = jax.nn.sigmoid(gate_pre)
    silu_gate = gate_pre * sigma
    hidden = (silu_gate * up_pre).astype(jnp.bfloat16)
    down_g = contract_rows(hidden, grads) * row_scale
    hidden_grad = contract_cols(grads, expert_down[0])
    gate_back = (hidden_grad * up_pre * sigma * (1.0 + gate_pre * (1.0 - sigma))).astype(
        jnp.bfloat16
    )
    up_back = (hidden_grad * silu_gate).astype(jnp.bfloat16)
    gate_g = contract_rows(inputs, gate_back) * row_scale
    up_g = contract_rows(inputs, up_back) * row_scale

    def partial_of(side):
        weight_g = lax.dynamic_slice_in_dim(expert_gate[0], side * share, share, 0)
        weight_u = lax.dynamic_slice_in_dim(expert_up[0], side * share, share, 0)
        return (contract_cols(gate_back, weight_g) + contract_cols(up_back, weight_u)).astype(
            jnp.bfloat16
        )

    arrived = lax.ppermute(
        partial_of(1 - half), "tp", [(i, n_tp - 1 - i) for i in range(n_tp)]
    )
    summed = (partial_of(half).astype(jnp.float32) + arrived.astype(jnp.float32)).astype(
        jnp.bfloat16
    )
    (returned,) = exchange([summed.reshape(blocks)], 2, relay=False)
    returned = returned.reshape(slots, share)
    grad_share = (grad_half.astype(jnp.float32) + contract_rows(pick, returned)).astype(
        jnp.bfloat16
    )
    input_grad = lax.all_gather(grad_share, "tp", axis=1, tiled=True)

    act_grad = jnp.dot(input_grad, proj_weight, preferred_element_type=jnp.float32)
    part = tok_rows // n_tp
    mine = lax.dynamic_slice_in_dim(input_grad, half * part, part, 0)
    mine = mine.reshape(part, n_sp, width // n_sp).transpose(1, 0, 2)
    (features,) = exchange([mine], 3, lanes=False)
    features = features.transpose(1, 0, 2, 3).reshape(n_sp * tok_rows, width // n_sp)
    token_scale = float(tok_rows * n_sp) ** (-0.5)
    proj_grad = contract_rows(features, all_activ) * token_scale

    norm_grad = act_grad * sig_norm * (1.0 + scaled * (1.0 - sig_norm)) * norm_gain[None, :]
    first, second = lax.psum(
        (jnp.sum(norm_grad, axis=1), jnp.sum(norm_grad * normed, axis=1)), "tp"
    )
    conv_grad = inv_std * (
        norm_grad - first[:, None] / channels - normed * (second[:, None] / channels)
    )
    reach = conv_taps.shape[0]
    rim = from_behind(conv_grad[: reach - 1].astype(jnp.bfloat16), "sp", -1).astype(jnp.float32)
    extended = jnp.concatenate([conv_grad, rim], axis=0)
    taps_float = conv_taps.astype(jnp.float32)
    mixed_grad = jnp.zeros_like(conv_grad)
    for lag in range(reach):
        mixed_grad = (
            mixed_grad + taps_float[reach - 1 - lag][None, :] * extended[lag : lag + tok_rows]
        )
    sig_gate = jax.nn.sigmoid(glu_gate.astype(jnp.float32))
    value_grad = (mixed_grad * sig_gate).astype(jnp.bfloat16)
    gate_side_grad = (
        mixed_grad * glu_value.astype(jnp.float32) * sig_gate * (1.0 - sig_gate)
    ).astype(jnp.bfloat16)
    return (
        input_grad,
        proj_grad,
        gate_g[None],
        up_g[None],
        down_g[None],
        value_grad,
        gate_side_grad,
    )


def solution(mesh):
    in_specs = (
        P("sp", None),
        P("sp", None),
        P("sp", None),
        P("sp", None),
        P("sp", "tp"),
        P("sp", "tp"),
        P("sp", "tp"),
        P(None, "tp"),
        P("tp"),
        P(None, "tp"),
        P("sp", None, "tp"),
        P("sp", None, "tp"),
        P("sp", "tp", None),
    )
    out_specs = (
        P("sp", None),
        P("sp", "tp"),
        P("sp", None, "tp"),
        P("sp", None, "tp"),
        P("sp", "tp", None),
        P("sp", "tp"),
        P("sp", "tp"),
    )
    return jax.shard_map(
        per_device, mesh=mesh, in_specs=in_specs, out_specs=out_specs, check_vma=False
    )
```

time: 348 us -> 287 us (0.82)
  Pallas kernels: 0 us -> 162 us
  blocking collectives: 108 us -> 8.69 us
  waiting for transfers between devices: 118 us -> 30.8 us
  local copies, waits for them, and re-layouts: 37.6 us -> 8.49 us
  matrix products: 43.1 us -> 52.6 us
  starting transfers between devices: 10.5 us -> 1.69 us
  other arithmetic: 16.1 us -> 7.39 us
    pallas_call x0 -> x3, Pallas kernels: none -> 162 us  [exchange(): pl.pallas_call(functools.partial(exchange_body, n, number, relay, lanes),...]
    all_to_all x2 -> x0, blocking collectives: 103 us -> none  [the longest x1 51.9 us: per_device(): lax.all_to_all(grad_share, 'sp', split_axis=0, concat_axis=0, tiled=True)]
    reduce_scatter x2 -> x0, waiting for transfers between devices: 81.8 us -> none  [the longest x1 68.9 us: per_device(): lax.psum_scatter(contract_rows(input_grad, activ) * token_scale, 'sp', sc...]
    all_to_all x1 -> x0, waiting for transfers between devices: 26.2 us -> none  [per_device(): lax.all_to_all(input_share, 'sp', split_axis=0, concat_axis=0, tiled=True)]
    gather x4 -> x0, local copies, waits for them, and re-layouts: 22.6 us -> none  [the longest x1 6.92 us: per_device(): returned[target].reshape(tok_rows, top_count, width).astype(jnp.float32)]
    all_gather x3 -> x1, waiting for transfers between devices: 9.82 us -> 30.8 us  [per_device(): all_activ = lax.all_gather(activ, 'sp', axis=0, tiled=True)]
    all_to_all x1 -> x0, starting transfers between devices: 8.39 us -> none  [per_device(): lax.all_to_all(input_share, 'sp', split_axis=0, concat_axis=0, tiled=True)]
    reduce_sum x2, other arithmetic: 6.51 us -> 0.31 us  [per_device(): jnp.sum(jnp.where(chosen[k], route_weights[:, k][None, :], 0.0), axis=1)]
  transfers between devices with their start and end apart: 7 -> 3, of which waited for: 5 -> 1; matrix products, arithmetic and copies ran while one was open for 13% -> 9% of each run, Pallas kernels for 0% -> 11%
where the time goes in v1:
time: 287 us; the launch traced here: 286 us
  Pallas kernels  162 us (56%)
  matrix products  52.6 us (18%)
  waiting for transfers between devices  30.8 us (11%)
  between operations  14.3 us (5%)
  blocking collectives  8.69 us (3%)
  local copies, waits for them, and re-layouts  8.49 us (3%)
  other arithmetic  7.39 us (3%)
    pallas_call x3, Pallas kernels, exchange(): pl.pallas_call(functools.partial(exchange_body, n, number, relay, lanes),...  162 us
    all_gather x1, waiting for transfers between devices, per_device(): all_activ = lax.all_gather(activ, 'sp', axis=0, tiled=True)  30.8 us
    dot_general x5, matrix products, contract_rows(): lax.dot_general(left, right, (((0,), (0,)), ((), ())), preferred_element_...  22 us
    dot_general x5, matrix products, contract_cols(): lax.dot_general(left, right, (((1,), (1,)), ((), ())), preferred_element_...  15 us
  transfers between devices with their start and end apart: 3, of which 1 were waited for; matrix products, arithmetic and copies ran while one was open for 9% of the time, Pallas kernels for 11%

profile of v1, /device:TPU:0, one launch (start us, length us, event | category | flops | bytes accessed | tf_op | source)
XLA Modules:
  0.0 286.5 jit_solution(6806697640445566975)
XLA Ops:
  7.2 0.0 copy-start
  7.2 0.0 copy-start.17
  7.2 0.0 all-gather.2.cloned.1.call-start
  7.2 0.9 fusion.157
  8.1 0.8 fusion.156
  8.9 0.2 select_reduce_fusion.3
  9.1 0.2 select_reduce_fusion.1
  9.3 0.2 select_reduce_fusion
  9.4 3.0 %convolution_convert_fusion = bf16[896,1024]{1,0:T(8,128)(2,1)} fusion(bf16[224,2048]{1,0:T(8,128)(2,1)} %param.14, s32[]{:T(128)S(6)} %select_n.27, s32[224]{0:T(256)S(1)} %get-tuple-element.65, s32[224]{0:T(256)S(1)} %get-tuple-element.66), kind=kOutput, calls=%fused_computation.47 | convolution fusion | flops 412561408 | bytes 2295556 | tf_op jit(solution)/shard_map/dot_general | solution.py:208
  12.5 2.0 multiply_convert_fusion
  14.5 79.1 %shard_map.180 = (bf16[16,56,2048]{2,1,0:T(8,128)(2,1)}, bf16[16,56,2048]{2,1,0:T(8,128)(2,1)}) custom-call(bf16[16,56,1024]{2,1,0:T(8,128)(2,1)} %bitcast.97, bf16[16,56,1024]{2,1,0:T(8,128)(2,1)} %bitcast.100), custom_call_target="tpu_custom_call" | custom-call | tf_op jit(solution)/shard_map/pallas_call | solution.py:156
  93.7 0.0 copy-start.5
  93.7 5.5 %fusion = f32[896,512]{1,0:T(8,128)} fusion(bf16[896,2048]{1,0:T(8,128)(2,1)} %bitcast.141, bf16[1,2048,512]{2,1,0:T(8,128)(2,1)S(1)} %copy-done), kind=kOutput, calls=%fused_computation.36 | convolution fusion | flops 1879048192 | bytes 7602176 | tf_op jit(solution)/shard_map/dot_general | solution.py:229
  99.2 3.3 %fusion.2 = f32[896,512]{1,0:T(8,128)} fusion(bf16[896,2048]{1,0:T(8,128)(2,1)S(1)} %bitcast.143, bf16[1,2048,512]{2,1,0:T(8,128)(2,1)S(1)} %copy-done.5), kind=kOutput, calls=%fused_computation.38 | convolution fusion | flops 1879048192 | bytes 7602176 | tf_op jit(solution)/shard_map/dot_general | solution.py:230
  102.5 6.4 %multiply_convert_fusion.2 = (bf16[896,512]{1,0:T(8,128)(2,1)S(1)}, bf16[896,512]{1,0:T(8,128)(2,1)S(1)}) fusion(f32[896,512]{1,0:T(8,128)} %fusion, f32[896,512]{1,0:T(8,128)} %fusion.2, bf16[896,2048]{1,0:T(8,128)(2,1)} %bitcast.139, bf16[1,512,2048]{2,1,0:T(8,128)(2,1)} %param.25), kind=kOutput, calls=%fused_computation.43 | convolution fusion | flops 1885011968 | bytes 11272192 | tf_op jit(solution)/shard_map/dot_general | solution.py:27
  108.9 0.0 copy-start.6
  108.9 1.2 fusion.11
  110.1 0.7 copy-done.6
  110.8 2.4 add_convert_fusion.1
  113.2 0.4 collective-permute-start
  113.6 0.2 convert_reduce_fusion
  113.7 3.6 %all-reduce.1 = (f32[224]{0:T(256)S(1)}, f32[224]{0:T(256)S(1)}) all-reduce(f32[224]{0:T(256)S(1)} %get-tuple-element.14, f32[224]{0:T(256)S(1)} %get-tuple-element.13), channel_id=1, replica_groups=mesh['sp'=16,'tp'=2] {'tp'}, use_global_device_ids=true, to_apply=%region_7.8 | all-reduce | flops 448 | bytes 3584 | tf_op jit(solution)/shard_map/psum | solution.py:219
  117.4 1.2 fusion.14
  118.5 0.0 copy-done.4
  118.5 0.7 copy-done.7
  119.2 4.0 %add_convert_fusion = bf16[896,1024]{1,0:T(8,128)(2,1)} fusion(bf16[896,1024]{1,0:T(8,128)(2,1)} %collective-permute-done, f32[896,1024]{1,0:T(8,128)S(1)} %fusion.14, bf16[896,512]{1,0:T(8,128)(2,1)S(1)} %copy-done.4, bf16[1,2048,512]{2,1,0:T(8,128)(2,1)S(1)} %copy-done.7, s32[]{:T(128)S(6)} %select_n.27), kind=kOutput, calls=%fused_computation.32 | convolution fusion | flops 945029120 | bytes 9306116 | tf_op jit(solution)/shard_map/dot_general | solution.py:27
  123.2 50.8 %shard_map.181 = bf16[16,56,1024]{2,1,0:T(8,128)(2,1)} custom-call(bf16[16,56,1024]{2,1,0:T(8,128)(2,1)} %bitcast.96), custom_call_target="tpu_custom_call" | custom-call | tf_op jit(solution)/shard_map/pallas_call | solution.py:156
  174.0 2.4 fusion.7
  176.5 2.6 all_gather.6
  179.1 1.5 fusion.152
  180.6 2.4 all-reduce
  183.1 2.1 fusion.126
  185.2 0.0 all-gather.2.cloned.1.call-update
  185.2 0.6 fusion.155
  185.9 0.7 fusion.154
  186.5 6.8 %multiply_bitcast_fusion.1 = f32[1,2048,512]{2,1,0:T(8,128)} fusion(bf16[896,2048]{1,0:T(8,128)(2,1)} %bitcast.142, bf16[896,512]{1,0:T(8,128)(2,1)} %copy-done.3), kind=kOutput, calls=%fused_computation.30 | convolution fusion | flops 1880096768 | bytes 8781824 | tf_op jit(solution)/shard_map/dot_general | solution.py:21
  193.4 4.5 %multiply_bitcast_fusion.2 = f32[1,2048,512]{2,1,0:T(8,128)} fusion(bf16[896,2048]{1,0:T(8,128)(2,1)S(1)} %bitcast.144, bf16[896,512]{1,0:T(8,128)(2,1)S(1)} %get-tuple-element.24), kind=kOutput, calls=%fused_computation.31 | convolution fusion | flops 1880096768 | bytes 8781824 | tf_op jit(solution)/shard_map/dot_general | solution.py:21
  197.8 4.6 %multiply_bitcast_fusion = f32[1,512,2048]{2,1,0:T(8,128)} fusion(bf16[896,2048]{1,0:T(8,128)(2,1)S(1)} %bitcast.140, f32[896,512]{1,0:T(8,128)S(1)} %copy-done.19, f32[896,512]{1,0:T(8,128)S(1)} %copy-done.18), kind=kOutput, calls=%fused_computation.29 | convolution fusion | flops 1882849280 | bytes 11534336 | tf_op jit(solution)/shard_map/dot_general | solution.py:21
  202.4 1.3 collective-permute-start.1
  203.7 0.9 bitcast_bitcast_fusion.refs_0_
  204.6 32.6 %shard_map.182 = bf16[2,16,112,128]{3,2,1,0:T(8,128)(2,1)} custom-call(bf16[16,112,128]{2,1,0:T(8,128)(2,1)} %bitcast_bitcast_fusion.refs_0_), custom_call_target="tpu_custom_call" | custom-call | tf_op jit(solution)/shard_map/pallas_call | solution.py:156
  237.1 0.0 copy-start.8
  237.1 2.2 copy.23
  239.4 4.0 %multiply_convert_fusion.5 = (bf16[224,512]{1,0:T(8,128)(2,1)}, f32[224,512]{1,0:T(8,128)S(1)}) fusion(bf16[224,512]{1,0:T(8,128)(2,1)S(1)} %copy-done.10, bf16[224,512]{1,0:T(8,128)(2,1)S(1)} %copy-done.8, f32[30,512]{1,0:T(8,128)S(1)} %convert_element_type.90, f32[224,512]{1,0:T(8,128)S(1)} %get-tuple-element.25, f32[512]{0:T(512)} %bitcast.113, ...), kind=kLoop, calls=%fused_computation.209 | loop fusion | flops 11583488 | bytes 1730560 | tf_op jit(solution)/shard_map/convert_element_type | solution.py:292
  243.4 0.8 multiply_convert_fusion.6
  244.2 30.8 %all-gather.2.cloned.1.call-done = bf16[3584,512]{1,0:T(8,128)(2,1)} async-done(((bf16[224,512]{1,0:T(8,128)(2,1)}), bf16[3584,512]{1,0:T(8,128)(2,1)}) %all-gather.2.cloned.1.call-update) | async-done | bytes 3670032 | tf_op jit(solution)/shard_map/all_gather | solution.py:227
  275.0 3.7 %convolution_multiply_fusion.1 = f32[128,512]{1,0:T(8,128)} fusion(bf16[3584,128]{1,0:T(8,128)(2,1)} %bitcast.98, bf16[3584,512]{1,0:T(8,128)(2,1)} %all-gather.2.cloned.1.call-done), kind=kOutput, calls=%fused_computation.53 | convolution fusion | flops 469827584 | bytes 4849664 | tf_op jit(solution)/shard_map/dot_general | solution.py:21
  278.7 0.9 copy.27
  (41 shorter events, 0.1 us)
Async XLA Ops:
  7.2 86.5 %copy-start = (bf16[1,2048,512]{2,1,0:T(8,128)(2,1)S(1)}, bf16[1,2048,512]{2,1,0:T(8,128)(2,1)}, u32[]{:S(2)}) copy-start(bf16[1,2048,512]{2,1,0:T(8,128)(2,1)} %param.23) | copy-start | bytes 6291460
  7.2 5.3 %copy-start.17 = (bf16[224,2048]{1,0:T(8,128)(2,1)S(1)}, bf16[224,2048]{1,0:T(8,128)(2,1)}, u32[]{:S(2)}) copy-start(bf16[224,2048]{1,0:T(8,128)(2,1)} %param.13) | copy-start | bytes 2752516
  7.2 267.8 %all-gather.2.cloned.1.call-start = ((), (), s32[]{:S(2)}) async-start(), calls=%async_computation | async-start | bytes 3899392 | tf_op jit(solution)/shard_map/all_gather | solution.py:227
  93.7 5.5 %copy-start.5 = (bf16[1,2048,512]{2,1,0:T(8,128)(2,1)S(1)}, bf16[1,2048,512]{2,1,0:T(8,128)(2,1)}, u32[]{:S(2)}) copy-start(bf16[1,2048,512]{2,1,0:T(8,128)(2,1)} %param.24) | copy-start | bytes 6291460
  93.7 5.5 %copy-start.14 = (bf16[16,56,2048]{2,1,0:T(8,128)(2,1)S(1)}, bf16[16,56,2048]{2,1,0:T(8,128)(2,1)}, u32[]{:S(2)}) copy-start(bf16[16,56,2048]{2,1,0:T(8,128)(2,1)} %get-tuple-element.10) | copy-start | bytes 11010052
  108.9 1.2 copy-start.3
  108.9 1.9 copy-start.6
  110.8 2.8 copy-start.9
  113.2 5.3 %collective-permute-start = (bf16[896,1024]{1,0:T(8,128)(2,1)}, bf16[896,1024]{1,0:T(8,128)(2,1)}, u32[]{:S(2)}, u32[]{:S(2)}) collective-permute-start(bf16[896,1024]{1,0:T(8,128)(2,1)} %add_convert_fusion.1), channel_id=1, source_target_pairs={{0,1},{1,0},{2,3},{3,2},{4,5},{5,4},{6,7},{7,6},{8,9},{9,8},{10,11... | collective-permute-start | bytes 5505032 | tf_op jit(solution)/shard_map/ppermute | solution.py:250
  117.4 1.2 copy-start.4
  117.4 1.9 copy-start.7
  174.0 5.1 %copy-start.12 = (f32[512]{0:T(512)S(1)}, f32[512]{0:T(512)}, u32[]{:S(2)}) copy-start(f32[512]{0:T(512)} %param.21) | copy-start | bytes 6148
  174.0 5.1 %copy-start.16 = (bf16[2048,512]{1,0:T(8,128)(2,1)S(1)}, bf16[2048,512]{1,0:T(8,128)(2,1)}, u32[]{:S(2)}) copy-start(bf16[2048,512]{1,0:T(8,128)(2,1)} %param.22) | copy-start | bytes 6291460
  179.1 1.5 copy-start.1
  179.1 6.1 %copy-start.11 = (bf16[31,512]{1,0:T(8,128)(2,1)S(1)}, bf16[31,512]{1,0:T(8,128)(2,1)}, u32[]{:S(2)}) copy-start(bf16[31,512]{1,0:T(8,128)(2,1)} %param.20) | copy-start | bytes 95236
  186.5 6.8 %copy-start.15 = (bf16[16,56,2048]{2,1,0:T(8,128)(2,1)S(1)}, bf16[16,56,2048]{2,1,0:T(8,128)(2,1)}, u32[]{:S(2)}) copy-start(bf16[16,56,2048]{2,1,0:T(8,128)(2,1)} %get-tuple-element.10) | copy-start | bytes 11010052
  193.4 4.5 %copy-start.13 = (bf16[16,56,2048]{2,1,0:T(8,128)(2,1)S(1)}, bf16[16,56,2048]{2,1,0:T(8,128)(2,1)}, u32[]{:S(2)}) copy-start(bf16[16,56,2048]{2,1,0:T(8,128)(2,1)} %get-tuple-element.9) | copy-start | bytes 11010052
  193.4 4.5 %copy-start.18 = (f32[896,512]{1,0:T(8,128)S(1)}, f32[896,512]{1,0:T(8,128)}, u32[]{:S(2)}) copy-start(f32[896,512]{1,0:T(8,128)} %fusion) | copy-start | bytes 5505028
  193.4 4.5 %copy-start.19 = (f32[896,512]{1,0:T(8,128)S(1)}, f32[896,512]{1,0:T(8,128)}, u32[]{:S(2)}) copy-start(f32[896,512]{1,0:T(8,128)} %fusion.2) | copy-start | bytes 5505028
  197.8 5.9 %copy-start.2 = (bf16[224,2048]{1,0:T(8,128)(2,1)S(1)}, bf16[224,2048]{1,0:T(8,128)(2,1)}, u32[]{:S(2)}) copy-start(bf16[224,2048]{1,0:T(8,128)(2,1)} %copy-done.1) | copy-start | bytes 2752516
  202.4 37.0 %collective-permute-start.1 = (bf16[30,512]{1,0:T(8,128)(2,1)S(1)}, bf16[30,512]{1,0:T(8,128)(2,1)S(1)}, u32[]{:S(2)}, u32[]{:S(2)}) collective-permute-start(bf16[30,512]{1,0:T(8,128)(2,1)S(1)} %slice.750), channel_id=1, source_target_pairs={{2,0},{4,2},{6,4},{8,6},{10,8},{12,10},{14,12},{16,14},{18,16},{20... | collective-permute-start | bytes 92168 | tf_op jit(solution)/shard_map/ppermute | solution.py:17
  237.1 2.3 copy-start.8
  237.1 2.3 copy-start.10
Sparse Core Ops, SparseCore 0:
  185.3 89.6 all-gather.1
